TPU v7x, 32 devices: a whole 2x2x4 slice. The times are simulated.
32 devices in a mesh: sp: 8 (over z, y), tp: 4 (over x, core).
Axes of the slice: x: 2, y: 2, z: 4, core: 2. Of those that a mesh axis runs over, the one named last changes fastest.
Arguments:
- resid: bfloat16 [2048, 2048], P(('sp', 'tp')), may hold values from -6 to 6
- query_a: bfloat16 [2048, 4, 128], P('sp', 'tp')
- key_a: bfloat16 [2048, 4, 128], P('sp', 'tp')
- value_a: bfloat16 [2048, 4, 128], P('sp', 'tp'), may hold values from -6 to 6
- query_b: bfloat16 [2048, 4, 256], P('sp', 'tp')
- key_b: bfloat16 [2048, 4, 256], P('sp', 'tp')
- value_b: bfloat16 [2048, 4, 128], P('sp', 'tp'), may hold values from -6 to 6
- lambda_a: float32 [4], P('tp'), may hold values from 0.3 to 0.8
- lambda_b: float32 [4], P('tp'), may hold values from 0.3 to 0.8
- head_gain: float32 [128], replicated, may hold values from 0.1 to 1.9
- out_weight: bfloat16 [1024, 2048], replicated, may hold values from -0.1875 to 0.1875
- norm_gain: float32 [2048], replicated, may hold values from 0.1 to 1.9
- expert_ids: int32 [2048, 4], P(('sp', 'tp')), may hold values from 0 to 31, all different within a row; in each aligned block of 64 rows (0 to 63, 64 to 127, ...) at most 16 rows name the same one
- expert_mix: float32 [2048, 4], P(('sp', 'tp')), may hold values from 0.2 to 1
- gate_experts: bfloat16 [32, 2048, 1024], P(('sp', 'tp')), may hold values from -0.125 to 0.125
- up_experts: bfloat16 [32, 2048, 1024], P(('sp', 'tp')), may hold values from -0.125 to 0.125
- down_experts: bfloat16 [32, 1024, 2048], P(('sp', 'tp')), may hold values from -0.1875 to 0.1875
- shared_gate: bfloat16 [2048, 512], replicated, may hold values from -0.125 to 0.125
- shared_up: bfloat16 [2048, 512], replicated, may hold values from -0.125 to 0.125
- shared_down: bfloat16 [512, 2048], replicated, may hold values from -0.25 to 0.25
Outputs:
- layer_out: bfloat16 [2048, 2048], P(('sp', 'tp'))
Inputs may be any that keep to these rules, and one draw needn't show every extreme that they name: `expert_ids`: in each aligned block of 64 rows (the rows of one device) no expert is named more than 16 times, a bound that some block reaches.
All inputs are finite; a program needn't handle non-finite values.
Results may differ from a plain program's by a relative error of at most 0.017.
Values may be sent and summed in bfloat16 or wider, within the bound.
No kernel may reach another device: no remote copies, remote signals or barrier semaphores. Data moves between devices by JAX's collectives and lax.ppermute only.
A program may use at most 128 MiB of HBM per device.

v0:
```python
import math
import jax
import jax.numpy as jnp
from jax import lax
from jax.sharding import PartitionSpec as P

NEG_FILL = -1e30
EPSILON = 1e-05
HEAD_SCALE = 0.8
KEY_SPAN = 2048


def swiglu_rows(row_set, w_gate, w_up, w_down):
    gate_val = jnp.dot(row_set, w_gate, preferred_element_type=jnp.float32)
    up_val = jnp.dot(row_set, w_up, preferred_element_type=jnp.float32)
    hidden = (jax.nn.silu(gate_val) * up_val).astype(jnp.bfloat16)
    return jnp.dot(hidden, w_down, preferred_element_type=jnp.float32)


def online_update(state, query_map, key_map, value_block, causal, scaling):
    row_top, denoms, numerator = state
    scores = (
        jnp.einsum("qhd,khd->hqk", query_map, key_map, preferred_element_type=jnp.float32) * scaling
    )
    scores = jnp.where(causal, scores, NEG_FILL)
    new_top = jnp.maximum(row_top, jnp.max(scores, axis=2))
    exponent = jnp.where(causal, jnp.exp(scores - new_top[:, :, None]), 0.0)
    shrink = jnp.exp(row_top - new_top)
    denoms = denoms * shrink + jnp.sum(exponent, axis=2)
    numerator = numerator * jnp.transpose(shrink)[:, :, None] + jnp.einsum(
        "hqk,khe->qhe",
        exponent.astype(jnp.bfloat16),
        value_block,
        preferred_element_type=jnp.float32,
    )
    return (new_top, denoms, numerator)


def group_update(states, queries, key_block, value_block, causal):
    map_width = queries.shape[2] // 2
    scaling = map_width ** (-0.5)
    first_state = online_update(
        states[0],
        queries[:, :, :map_width],
        key_block[:, :, :map_width],
        value_block,
        causal,
        scaling,
    )
    second_state = online_update(
        states[1],
        queries[:, :, map_width:],
        key_block[:, :, map_width:],
        value_block,
        causal,
        scaling,
    )
    return (first_state, second_state)


def empty_state(query_rows, head_count, value_width):
    single = (
        jnp.full((head_count, query_rows), NEG_FILL, jnp.float32),
        jnp.zeros((head_count, query_rows), jnp.float32),
        jnp.zeros((query_rows, head_count, value_width), jnp.float32),
    )
    return (single, single)


def finish_group(states, lambdas, head_gain):
    first_out = states[0][2] / jnp.transpose(states[0][1])[:, :, None]
    second_out = states[1][2] / jnp.transpose(states[1][1])[:, :, None]
    differ = first_out - lambdas[None, :, None] * second_out
    scale_rms = lax.rsqrt(jnp.mean(differ * differ, axis=2, keepdims=True) + EPSILON)
    return (differ * scale_rms * head_gain[None, None, :] * HEAD_SCALE).astype(jnp.bfloat16)


def per_device(
    resid,
    query_a,
    key_a,
    value_a,
    query_b,
    key_b,
    value_b,
    lambda_a,
    lambda_b,
    head_gain,
    out_weight,
    norm_gain,
    expert_ids,
    expert_mix,
    gate_experts,
    up_experts,
    down_experts,
    shared_gate,
    shared_up,
    shared_down,
):
    query_rows = query_a.shape[0]
    value_width = value_a.shape[2]
    query_pos = lax.axis_index("sp") * query_rows + jnp.arange(query_rows, dtype=jnp.int32)
    start_state = (
        empty_state(query_rows, query_a.shape[1], value_width),
        empty_state(query_rows, query_b.shape[1], value_width),
    )
    key_piece_a = lax.all_gather(key_a, "sp", axis=0, tiled=True)
    value_piece_a = lax.all_gather(value_a, "sp", axis=0, tiled=True)
    key_piece_b = lax.all_gather(key_b, "sp", axis=0, tiled=True)
    value_piece_b = lax.all_gather(value_b, "sp", axis=0, tiled=True)
    piece_rows = key_piece_a.shape[0]
    step_rows = math.gcd(piece_rows, KEY_SPAN)

    def one_step(step_index, inner_state):
        begin_row = step_index * step_rows
        key_pos = begin_row + jnp.arange(step_rows, dtype=jnp.int32)
        causal = (key_pos[None, :] <= query_pos[:, None])[None]
        part_a = group_update(
            inner_state[0],
            query_a,
            lax.dynamic_slice_in_dim(key_piece_a, begin_row, step_rows, 0),
            lax.dynamic_slice_in_dim(value_piece_a, begin_row, step_rows, 0),
            causal,
        )
        part_b = group_update(
            inner_state[1],
            query_b,
            lax.dynamic_slice_in_dim(key_piece_b, begin_row, step_rows, 0),
            lax.dynamic_slice_in_dim(value_piece_b, begin_row, step_rows, 0),
            causal,
        )
        return (part_a, part_b)

    state_a, state_b = lax.fori_loop(0, piece_rows // step_rows, one_step, start_state)
    heads_a = finish_group(state_a, lambda_a, head_gain)
    heads_b = finish_group(state_b, lambda_b, head_gain)
    tok_dev = resid.shape[0]
    back_a, back_b = (
        lax.all_to_all(heads_a, "tp", split_axis=0, concat_axis=1, tiled=True),
        lax.all_to_all(heads_b, "tp", split_axis=0, concat_axis=1, tiled=True),
    )
    joined = jnp.concatenate([back_a.reshape(tok_dev, -1), back_b.reshape(tok_dev, -1)], axis=1)
    project = jnp.dot(joined, out_weight, preferred_element_type=jnp.float32)
    middle = (resid.astype(jnp.float32) + project).astype(jnp.bfloat16)
    middle_f = middle.astype(jnp.float32)
    normed = (
        middle_f
        * lax.rsqrt(jnp.mean(middle_f * middle_f, axis=1, keepdims=True) + EPSILON)
        * norm_gain[None, :]
    ).astype(jnp.bfloat16)
    shared = swiglu_rows(normed, shared_gate, shared_up, shared_down)
    top_count = expert_ids.shape[1]
    model_width = normed.shape[1]
    sp_count = lax.axis_size("sp")
    tp_count = lax.axis_size("tp")
    expert_total = sp_count * tp_count
    pair_count = tok_dev * top_count
    capacity = max(2, 2 * pair_count // expert_total)
    flat_ids = expert_ids.reshape(-1)
    one_hot = (flat_ids[:, None] == jnp.arange(expert_total, dtype=jnp.int32)[None, :]).astype(
        jnp.int32
    )
    pair_rank = jnp.sum((jnp.cumsum(one_hot, axis=0) - one_hot) * one_hot, axis=1)
    pair_token = jnp.arange(pair_count, dtype=jnp.int32) // top_count
    send_rows = (
        jnp.zeros((expert_total, capacity, model_width), jnp.bfloat16)
        .at[flat_ids, pair_rank]
        .set(normed[pair_token])
    )
    arrived = lax.all_to_all(send_rows, ("sp", "tp"), split_axis=0, concat_axis=0, tiled=True)
    arrived_shape = arrived.shape
    flat_rows = arrived.reshape(-1, arrived_shape[-1])
    result = swiglu_rows(flat_rows, gate_experts[0], up_experts[0], down_experts[0]).astype(
        jnp.bfloat16
    )
    finished = result.reshape(arrived_shape)
    returned = lax.all_to_all(finished, ("sp", "tp"), split_axis=0, concat_axis=0, tiled=True)
    chosen = returned[flat_ids, pair_rank].reshape(tok_dev, top_count, model_width)
    routed = jnp.sum(chosen.astype(jnp.float32) * expert_mix[:, :, None], axis=1)
    return (middle_f + shared + routed).astype(jnp.bfloat16)


def solution(mesh):
    in_specs = (
        P(("sp", "tp"), None),
        P("sp", "tp", None),
        P("sp", "tp", None),
        P("sp", "tp", None),
        P("sp", "tp", None),
        P("sp", "tp", None),
        P("sp", "tp", None),
        P("tp"),
        P("tp"),
        P(),
        P(),
        P(),
        P(("sp", "tp"), None),
        P(("sp", "tp"), None),
        P(("sp", "tp"), None, None),
        P(("sp", "tp"), None, None),
        P(("sp", "tp"), None, None),
        P(),
        P(),
        P(),
    )
    out_specs = P(("sp", "tp"), None)
    return jax.shard_map(
        per_device, mesh=mesh, in_specs=in_specs, out_specs=out_specs, check_vma=False
    )
```

profile of v0, /device:TPU:0, one launch (start us, length us, event | category | flops | bytes accessed | tf_op | source)
XLA Modules:
  0.0 333.9 jit_solution(18437636033774966400)
XLA Ops:
  6.5 0.7 all-gather.2.cloned.1.call-update
  7.3 33.6 %all_gather.12 = bf16[2048,1,128]{2,0,1:T(8,128)(2,1)S(1)} all-gather(bf16[256,1,128]{2,0,1:T(8,128)(2,1)} %param.22), channel_id=1, replica_groups=mesh['sp'=8,'tp'=4] {'sp'}, dimensions={0}, use_global_device_ids=true | all-gather | bytes 589824 | tf_op jit(solution)/shard_map/all_gather | solution.py:107
  40.9 0.8 copy.35
  44.2 2.8 fusion.88
  47.0 1.8 fusion.89
  48.9 31.4 %all_gather.15 = bf16[2048,1,128]{2,0,1:T(8,128)(2,1)S(1)} all-gather(bf16[256,1,128]{2,0,1:T(8,128)(2,1)S(1)} %copy-done.5), channel_id=1, replica_groups=mesh['sp'=8,'tp'=4] {'sp'}, dimensions={0}, use_global_device_ids=true | all-gather | bytes 589824 | tf_op jit(solution)/shard_map/all_gather | solution.py:110
  80.3 31.5 %all_gather.13 = bf16[2048,1,128]{2,0,1:T(8,128)(2,1)S(1)} all-gather(bf16[256,1,128]{2,0,1:T(8,128)(2,1)S(1)} %copy-done.6), channel_id=1, replica_groups=mesh['sp'=8,'tp'=4] {'sp'}, dimensions={0}, use_global_device_ids=true | all-gather | bytes 589824 | tf_op jit(solution)/shard_map/all_gather | solution.py:108
  111.8 1.8 fusion.91
  113.6 1.8 fusion.90
  115.4 2.1 fusion.19
  121.0 0.7 reduce.22
  122.5 3.3 all-to-all-start.1
  125.8 0.7 reduce.23
  127.3 2.6 all-to-all-done.1
  129.9 3.3 all-to-all-start
  133.3 3.9 %all-to-all-done = bf16[4,2,4096]{2,1,0:T(2,128)(2,1)S(1)} async-done(((bf16[4,2,4096]{2,1,0:T(2,128)(2,1)}), bf16[4,2,4096]{2,1,0:T(2,128)(2,1)S(1)}, u32[]{:S(2)}, u32[]{:S(2)}) %all-to-all-start) | async-done | bytes 65568 | tf_op jit(solution)/shard_map/all_to_all | solution.py:139
  137.4 3.2 multiply_reduce_fusion.1
  140.7 2.3 gather_fusion
  143.1 1.6 broadcast_in_dim.49
  144.7 46.2 %scatter_fusion = bf16[32,16,2048]{2,1,0:T(8,128)(2,1)} fusion(bf16[32,16,2048]{2,1,0:T(8,128)(2,1)} %broadcast_in_dim.49, s32[256]{0:T(256)S(1)} %bitcast.169, bf16[256,2048]{1,0:T(8,128)(2,1)} %gather_fusion), kind=kCustom, calls=%fused_computation.2 | custom fusion | bytes 3147776 | tf_op jit(solution)/shard_map/scatter | solution.py:168
  190.9 53.7 %all_to_all.40 = bf16[32,16,2048]{2,1,0:T(8,128)(2,1)S(1)} all-to-all(bf16[32,16,2048]{2,1,0:T(8,128)(2,1)} %scatter_fusion), channel_id=1, replica_groups=mesh['sp'=8,'tp'=4] {'sp','tp'}, dimensions={0} | all-to-all | bytes 4194304 | tf_op jit(solution)/shard_map/all_to_all | solution.py:170
  244.6 1.3 copy-done.3
  246.0 3.6 %fusion.4 = f32[512,1024]{1,0:T(8,128)} fusion(bf16[512,2048]{1,0:T(8,128)(2,1)S(1)} %bitcast.171, bf16[1,2048,1024]{2,1,0:T(8,128)(2,1)S(1)} %copy-done.10), kind=kOutput, calls=%fused_computation.7 | convolution fusion | flops 2147483648 | bytes 8388608 | tf_op jit(solution)/shard_map/dot_general | solution.py:14
  249.6 10.6 %fusion.6 = bf16[512,2048]{1,0:T(8,128)(2,1)} fusion(bf16[1,1024,2048]{2,1,0:T(8,128)(2,1)} %param.36, f32[512,1024]{1,0:T(8,128)} %fusion.4, bf16[512,2048]{1,0:T(8,128)(2,1)} %bitcast.172, bf16[1,2048,1024]{2,1,0:T(8,128)(2,1)} %param.35), kind=kOutput, calls=%fused_computation.9 | convolution fusion | flops 4299161600 | bytes 14680064 | tf_op jit(solution)/shard_map/dot_general | solution.py:17
  260.2 3.8 %all-to-all-start.3 = ((bf16[32,16,2048]{2,1,0:T(8,128)(2,1)}), bf16[32,16,2048]{2,1,0:T(8,128)(2,1)}, u32[]{:S(2)}, u32[]{:S(2)}) async-start(bf16[32,16,2048]{2,1,0:T(8,128)(2,1)} %bitcast.170), calls=%async_computation.3 | async-start | bytes 4194304 | tf_op jit(solution)/shard_map/all_to_all | solution.py:177
  264.0 0.7 copy.39
  264.7 2.1 fusion.92
  266.8 45.9 %all-to-all-done.3 = bf16[32,16,2048]{2,1,0:T(8,128)(2,1)} async-done(((bf16[32,16,2048]{2,1,0:T(8,128)(2,1)}), bf16[32,16,2048]{2,1,0:T(8,128)(2,1)}, u32[]{:S(2)}, u32[]{:S(2)}) %all-to-all-start.3) | async-done | bytes 2097184 | tf_op jit(solution)/shard_map/all_to_all | solution.py:177
  312.7 5.1 %gather_fusion.1 = bf16[256,2048]{1,0:T(8,128)(2,1)} fusion(bf16[32,16,2048]{2,1,0:T(8,128)(2,1)} %all-to-all-done.3, s32[256]{0:T(256)S(1)} %bitcast.168), kind=kCustom, calls=%fused_computation.1 | custom fusion | bytes 2099200 | tf_op jit(solution)/shard_map/gather | solution.py:178
  317.9 2.7 reshape.410
  320.6 3.2 multiply_reduce_fusion
  323.8 3.2 fusion.14
  (68 shorter events, 6.7 us)
Async XLA Ops:
  6.5 317.3 %copy-start = (bf16[512,2048]{1,0:T(8,128)(2,1)S(1)}, bf16[512,2048]{1,0:T(8,128)(2,1)}, u32[]{:S(2)}) copy-start(bf16[512,2048]{1,0:T(8,128)(2,1)} %param.39) | copy-start | bytes 6291460
  6.5 40.5 %copy-start.12 = (bf16[256,1,128]{2,0,1:T(8,128)(2,1)S(1)}, bf16[256,1,128]{2,0,1:T(8,128)(2,1)}, u32[]{:S(2)}) copy-start(bf16[256,1,128]{2,0,1:T(8,128)(2,1)} %param.21) | copy-start | bytes 196612
  6.5 105.2 %all-gather.2.cloned.1.call-start = ((), (), s32[]{:S(2)}) async-start(), calls=%async_computation.4 | async-start | bytes 1179648 | tf_op jit(solution)/shard_map/all_gather | solution.py:109
  47.0 1.9 copy-start.5
  47.0 33.3 %copy-start.6 = (bf16[256,1,128]{2,0,1:T(8,128)(2,1)S(1)}, bf16[256,1,128]{2,0,1:T(8,128)(2,1)}, u32[]{:S(2)}) copy-start(bf16[256,1,128]{2,0,1:T(8,128)(2,1)} %param.23) | copy-start | bytes 196612
  47.0 64.8 %copy-start.11 = (bf16[256,1,256]{2,0,1:T(8,128)(2,1)S(1)}, bf16[256,1,256]{2,0,1:T(8,128)(2,1)}, u32[]{:S(2)}) copy-start(bf16[256,1,256]{2,0,1:T(8,128)(2,1)} %param.24) | copy-start | bytes 393220
  111.8 3.6 %copy-start.2 = (f32[256,2048]{1,0:T(8,128)S(1)}, f32[256,2048]{1,0:T(8,128)}, u32[]{:S(2)}) copy-start(f32[256,2048]{1,0:T(8,128)} %get-tuple-element.62) | copy-start | bytes 6291460
  113.6 1.8 copy-start.1
  119.6 0.7 copy-start.9
  120.3 17.1 %copy-start.4 = (bf16[64,2048]{1,0:T(8,128)(2,1)S(1)}, bf16[64,2048]{1,0:T(8,128)(2,1)}, u32[]{:S(2)}) copy-start(bf16[64,2048]{1,0:T(8,128)(2,1)} %param.20) | copy-start | bytes 786436
  122.5 7.4 %all-to-all-start.1 = ((bf16[4,2,4096]{2,1,0:T(2,128)(2,1)}), bf16[4,2,4096]{2,1,0:T(2,128)(2,1)S(1)}, u32[]{:S(2)}, u32[]{:S(2)}) async-start(bf16[4,2,4096]{2,1,0:T(2,128)(2,1)} %reshape.432), calls=%async_computation.1 | async-start | bytes 131072 | tf_op jit(solution)/shard_map/all_to_all | solution.py:140
  129.9 7.4 %all-to-all-start = ((bf16[4,2,4096]{2,1,0:T(2,128)(2,1)}), bf16[4,2,4096]{2,1,0:T(2,128)(2,1)S(1)}, u32[]{:S(2)}, u32[]{:S(2)}) async-start(bf16[4,2,4096]{2,1,0:T(2,128)(2,1)} %reshape.434), calls=%async_computation | async-start | bytes 131072 | tf_op jit(solution)/shard_map/all_to_all | solution.py:139
  137.4 3.2 copy-start.7
  190.9 55.0 %copy-start.10 = (bf16[1,2048,1024]{2,1,0:T(8,128)(2,1)S(1)}, bf16[1,2048,1024]{2,1,0:T(8,128)(2,1)}, u32[]{:S(2)}) copy-start(bf16[1,2048,1024]{2,1,0:T(8,128)(2,1)} %param.34) | copy-start | bytes 12582916
  244.6 1.3 copy-start.3
  260.2 3.8 %copy-start.8 = (f32[64,4]{0,1:T(4,128)S(1)}, f32[64,4]{0,1:T(4,128)}, u32[]{:S(2)}) copy-start(f32[64,4]{0,1:T(4,128)} %param.33) | copy-start | bytes 3076
  260.2 52.5 %all-to-all-start.3 = ((bf16[32,16,2048]{2,1,0:T(8,128)(2,1)}), bf16[32,16,2048]{2,1,0:T(8,128)(2,1)}, u32[]{:S(2)}, u32[]{:S(2)}) async-start(bf16[32,16,2048]{2,1,0:T(8,128)(2,1)} %bitcast.170), calls=%async_computation.3 | async-start | bytes 4194304 | tf_op jit(solution)/shard_map/all_to_all | solution.py:177
Sparse Core Ops, SparseCore 0:
  9.5 43.6 all-gather.1
where the time goes:
time: 336 us; the launch traced here: 334 us
  blocking collectives  150 us (45%)
  local copies, waits for them, and re-layouts  63.9 us (19%)
  waiting for transfers between devices  53.1 us (16%)
  matrix products  33.6 us (10%)
  between operations  15.1 us (4%)
  starting transfers between devices  10.4 us (3%)
  other arithmetic  7.7 us (2%)
    all_to_all x1, blocking collectives, per_device(): lax.all_to_all(send_rows, ('sp', 'tp'), split_axis=0, concat_axis=0, tile...  53.7 us
    scatter x1, local copies, waits for them, and re-layouts, per_device(): send_rows = jnp.zeros((expert_total, capacity, model_width), jnp.bfloat16...  46.2 us
    all_to_all x1, waiting for transfers between devices, per_device(): lax.all_to_all(finished, ('sp', 'tp'), split_axis=0, concat_axis=0, tiled...  45.9 us
    all_gather x1, blocking collectives, per_device(): key_piece_a = lax.all_gather(key_a, 'sp', axis=0, tiled=True)  33.6 us
    all_gather x1, blocking collectives, per_device(): value_piece_a = lax.all_gather(value_a, 'sp', axis=0, tiled=True)  31.5 us
    all_gather x1, blocking collectives, per_device(): value_piece_b = lax.all_gather(value_b, 'sp', axis=0, tiled=True)  31.4 us
    dot_general x2, matrix products, swiglu_rows(): return jnp.dot(hidden, w_down, preferred_element_type=jnp.float32)  13.8 us
    dot_general x4, matrix products, online_update(): jnp.einsum('qhd,khd->hqk', query_map, key_map, preferred_element_type=jnp...  8.17 us
  transfers between devices with their start and end apart: 4, of which 3 were waited for; matrix products, arithmetic and copies ran while one was open for 3% of the time, Pallas kernels for 0%

commit v1 on v0

--- a/solution.py
+++ b/solution.py
@@ -104,7 +104,12 @@
         empty_state(query_rows, query_a.shape[1], value_width),
         empty_state(query_rows, query_b.shape[1], value_width),
     )
-    key_piece_a = lax.all_gather(key_a, "sp", axis=0, tiled=True)
+    ring = [key_a]
+    for hop in range(7):
+        ring.append(lax.ppermute(ring[-1], "sp", [(dev, (dev + 1) % 8) for dev in range(8)]))
+    key_piece_a = jnp.roll(
+        jnp.concatenate(ring[::-1], axis=0), (lax.axis_index("sp") + 1) * ring[0].shape[0], axis=0
+    )
     value_piece_a = lax.all_gather(value_a, "sp", axis=0, tiled=True)
     key_piece_b = lax.all_gather(key_b, "sp", axis=0, tiled=True)
     value_piece_b = lax.all_gather(value_b, "sp", axis=0, tiled=True)

time: 336 us -> 340 us (1.012)
  blocking collectives: 150 us -> 116 us
  waiting for transfers between devices: 53.1 us -> 84.5 us
  starting transfers between devices: 10.4 us -> 15.3 us
  local copies, waits for them, and re-layouts: 63.9 us -> 67.4 us
    all_gather x1 -> x0, blocking collectives: 33.6 us -> none  [per_device(): key_piece_a = lax.all_gather(key_a, 'sp', axis=0, tiled=True)]
    ppermute x0 -> x7, waiting for transfers between devices: none -> 32.1 us  [per_device(): lax.ppermute(ring[-1], 'sp', [(dev, (dev + 1) % 8) for dev in range(8)])]
    ppermute x0 -> x7, starting transfers between devices: none -> 5.04 us  [per_device(): lax.ppermute(ring[-1], 'sp', [(dev, (dev + 1) % 8) for dev in range(8)])]
    unnamed x38 -> x51, local copies, waits for them, and re-layouts: 4.57 us -> 8.14 us
  transfers between devices with their start and end apart: 4 -> 11, of which waited for: 3 -> 8; matrix products, arithmetic and copies ran while one was open for 3% -> 4% of each run, Pallas kernels for 0% -> 0%
where the time goes in v1:
time: 340 us; the launch traced here: 338 us
  blocking collectives  116 us (34%)
  waiting for transfers between devices  84.5 us (25%)
  local copies, waits for them, and re-layouts  67.4 us (20%)
  matrix products  32.2 us (9%)
  starting transfers between devices  15.3 us (4%)
  between operations  15.1 us (4%)
  other arithmetic  7.12 us (2%)
    all_to_all x1, blocking collectives, per_device(): lax.all_to_all(send_rows, ('sp', 'tp'), split_axis=0, concat_axis=0, tile...  51.9 us
    scatter x1, local copies, waits for them, and re-layouts, per_device(): send_rows = jnp.zeros((expert_total, capacity, model_width), jnp.bfloat16...  46.2 us
    all_to_all x1, waiting for transfers between devices, per_device(): lax.all_to_all(finished, ('sp', 'tp'), split_axis=0, concat_axis=0, tiled...  45.9 us
    all_gather x1, blocking collectives, per_device(): value_piece_b = lax.all_gather(value_b, 'sp', axis=0, tiled=True)  32.2 us
    ppermute x7, waiting for transfers between devices, per_device(): lax.ppermute(ring[-1], 'sp', [(dev, (dev + 1) % 8) for dev in range(8)])  32.1 us
    all_gather x1, blocking collectives, per_device(): value_piece_a = lax.all_gather(value_a, 'sp', axis=0, tiled=True)  31.8 us
    dot_general x2, matrix products, swiglu_rows(): return jnp.dot(hidden, w_down, preferred_element_type=jnp.float32)  13.8 us
    unnamed x51, local copies, waits for them, and re-layouts  8.14 us
  transfers between devices with their start and end apart: 11, of which 8 were waited for; matrix products, arithmetic and copies ran while one was open for 4% of the time, Pallas kernels for 0%

profile of v1, /device:TPU:0, one launch (start us, length us, event | category | flops | bytes accessed | tf_op | source)
XLA Modules:
  0.0 337.7 jit_solution(4283059583685503015)
XLA Ops:
  6.5 3.0 collective-permute-start
  9.6 32.2 %all_gather.11 = bf16[2048,1,128]{2,0,1:T(8,128)(2,1)S(1)} all-gather(bf16[256,1,128]{2,0,1:T(8,128)(2,1)} %param.26), channel_id=1, replica_groups=mesh['sp'=8,'tp'=4] {'sp'}, dimensions={0}, use_global_device_ids=true | all-gather | bytes 589824 | tf_op jit(solution)/shard_map/all_gather | solution.py:115
  42.8 31.8 %all_gather.9 = bf16[2048,1,128]{2,0,1:T(8,128)(2,1)S(1)} all-gather(bf16[256,1,128]{2,0,1:T(8,128)(2,1)} %param.23), channel_id=1, replica_groups=mesh['sp'=8,'tp'=4] {'sp'}, dimensions={0}, use_global_device_ids=true | all-gather | bytes 589824 | tf_op jit(solution)/shard_map/all_gather | solution.py:113
  77.3 5.2 %collective-permute-done.2 = bf16[256,1,128]{2,0,1:T(8,128)(2,1)S(1)} collective-permute-done((bf16[256,1,128]{2,0,1:T(8,128)(2,1)S(1)}, bf16[256,1,128]{2,0,1:T(8,128)(2,1)S(1)}, u32[]{:S(2)}, u32[]{:S(2)}) %collective-permute-start.2) | collective-permute-done | bytes 65568 | tf_op jit(solution)/shard_map/ppermute | solution.py:109
  82.8 6.7 %collective-permute-done.3 = bf16[256,1,128]{2,0,1:T(8,128)(2,1)S(1)} collective-permute-done((bf16[256,1,128]{2,0,1:T(8,128)(2,1)S(1)}, bf16[256,1,128]{2,0,1:T(8,128)(2,1)S(1)}, u32[]{:S(2)}, u32[]{:S(2)}) %collective-permute-start.3) | collective-permute-done | bytes 65568 | tf_op jit(solution)/shard_map/ppermute | solution.py:109
  89.6 7.0 %collective-permute-done.4 = bf16[256,1,128]{2,0,1:T(8,128)(2,1)} collective-permute-done((bf16[256,1,128]{2,0,1:T(8,128)(2,1)S(1)}, bf16[256,1,128]{2,0,1:T(8,128)(2,1)}, u32[]{:S(2)}, u32[]{:S(2)}) %collective-permute-start.4) | collective-permute-done | bytes 65568 | tf_op jit(solution)/shard_map/ppermute | solution.py:109
  97.9 5.9 %collective-permute-done.5 = bf16[256,1,128]{2,0,1:T(8,128)(2,1)} collective-permute-done((bf16[256,1,128]{2,0,1:T(8,128)(2,1)}, bf16[256,1,128]{2,0,1:T(8,128)(2,1)}, u32[]{:S(2)}, u32[]{:S(2)}) %collective-permute-start.5) | collective-permute-done | bytes 65568 | tf_op jit(solution)/shard_map/ppermute | solution.py:109
  103.9 7.2 %collective-permute-done.6 = bf16[256,1,128]{2,0,1:T(8,128)(2,1)S(1)} collective-permute-done((bf16[256,1,128]{2,0,1:T(8,128)(2,1)}, bf16[256,1,128]{2,0,1:T(8,128)(2,1)S(1)}, u32[]{:S(2)}, u32[]{:S(2)}) %collective-permute-start.6) | collective-permute-done | bytes 65568 | tf_op jit(solution)/shard_map/ppermute | solution.py:109
  114.7 1.9 fusion.99
  116.6 1.9 fusion.98
  118.5 1.7 fusion.101
  120.2 1.7 fusion.100
  122.0 1.5 fusion.21
  128.1 3.3 all-to-all-start.1
  132.9 2.6 all-to-all-done.1
  135.5 3.3 all-to-all-start
  139.0 3.9 %all-to-all-done = bf16[4,2,4096]{2,1,0:T(2,128)(2,1)S(1)} async-done(((bf16[4,2,4096]{2,1,0:T(2,128)(2,1)}), bf16[4,2,4096]{2,1,0:T(2,128)(2,1)S(1)}, u32[]{:S(2)}, u32[]{:S(2)}) %all-to-all-start) | async-done | bytes 65568 | tf_op jit(solution)/shard_map/all_to_all | solution.py:144
  143.1 3.2 multiply_reduce_fusion.1
  146.4 2.3 gather_fusion
  148.7 1.6 broadcast_in_dim.49
  150.3 46.2 %scatter_fusion = bf16[32,16,2048]{2,1,0:T(8,128)(2,1)} fusion(bf16[32,16,2048]{2,1,0:T(8,128)(2,1)} %broadcast_in_dim.49, s32[256]{0:T(256)S(1)} %bitcast.177, bf16[256,2048]{1,0:T(8,128)(2,1)} %gather_fusion), kind=kCustom, calls=%fused_computation.2 | custom fusion | bytes 3147776 | tf_op jit(solution)/shard_map/scatter | solution.py:173
  196.6 51.9 %all_to_all.40 = bf16[32,16,2048]{2,1,0:T(8,128)(2,1)S(1)} all-to-all(bf16[32,16,2048]{2,1,0:T(8,128)(2,1)} %scatter_fusion), channel_id=1, replica_groups=mesh['sp'=8,'tp'=4] {'sp','tp'}, dimensions={0} | all-to-all | bytes 4194304 | tf_op jit(solution)/shard_map/all_to_all | solution.py:175
  248.5 1.3 copy-done.3
  249.8 3.6 %fusion.4 = f32[512,1024]{1,0:T(8,128)} fusion(bf16[512,2048]{1,0:T(8,128)(2,1)S(1)} %bitcast.179, bf16[1,2048,1024]{2,1,0:T(8,128)(2,1)S(1)} %copy-done.9), kind=kOutput, calls=%fused_computation.7 | convolution fusion | flops 2147483648 | bytes 8388608 | tf_op jit(solution)/shard_map/dot_general | solution.py:14
  253.4 10.6 %fusion.6 = bf16[512,2048]{1,0:T(8,128)(2,1)} fusion(bf16[1,1024,2048]{2,1,0:T(8,128)(2,1)} %param.36, f32[512,1024]{1,0:T(8,128)} %fusion.4, bf16[512,2048]{1,0:T(8,128)(2,1)} %bitcast.180, bf16[1,2048,1024]{2,1,0:T(8,128)(2,1)} %param.35), kind=kOutput, calls=%fused_computation.9 | convolution fusion | flops 4299161600 | bytes 14680064 | tf_op jit(solution)/shard_map/dot_general | solution.py:17
  264.0 3.7 %all-to-all-start.3 = ((bf16[32,16,2048]{2,1,0:T(8,128)(2,1)}), bf16[32,16,2048]{2,1,0:T(8,128)(2,1)}, u32[]{:S(2)}, u32[]{:S(2)}) async-start(bf16[32,16,2048]{2,1,0:T(8,128)(2,1)} %bitcast.178), calls=%async_computation.3 | async-start | bytes 4194304 | tf_op jit(solution)/shard_map/all_to_all | solution.py:182
  268.5 2.1 fusion.102
  270.5 45.9 %all-to-all-done.3 = bf16[32,16,2048]{2,1,0:T(8,128)(2,1)} async-done(((bf16[32,16,2048]{2,1,0:T(8,128)(2,1)}), bf16[32,16,2048]{2,1,0:T(8,128)(2,1)}, u32[]{:S(2)}, u32[]{:S(2)}) %all-to-all-start.3) | async-done | bytes 2097184 | tf_op jit(solution)/shard_map/all_to_all | solution.py:182
  316.5 5.1 %gather_fusion.1 = bf16[256,2048]{1,0:T(8,128)(2,1)} fusion(bf16[32,16,2048]{2,1,0:T(8,128)(2,1)} %all-to-all-done.3, s32[256]{0:T(256)S(1)} %bitcast.176), kind=kCustom, calls=%fused_computation.1 | custom fusion | bytes 2099200 | tf_op jit(solution)/shard_map/gather | solution.py:183
  321.6 2.7 reshape.410
  324.4 3.2 multiply_reduce_fusion
  327.6 3.2 fusion.16
  (95 shorter events, 14.9 us)
Async XLA Ops:
  6.5 321.0 %copy-start = (bf16[512,2048]{1,0:T(8,128)(2,1)S(1)}, bf16[512,2048]{1,0:T(8,128)(2,1)}, u32[]{:S(2)}) copy-start(bf16[512,2048]{1,0:T(8,128)(2,1)} %param.39) | copy-start | bytes 6291460
  6.5 106.3 %copy-start.4 = (bf16[256,1,128]{2,0,1:T(8,128)(2,1)S(1)}, bf16[256,1,128]{2,0,1:T(8,128)(2,1)}, u32[]{:S(2)}) copy-start(bf16[256,1,128]{2,0,1:T(8,128)(2,1)} %param.22) | copy-start | bytes 196612
  6.5 111.9 %all-gather.2.cloned.1.call-start = ((), (), s32[]{:S(2)}) async-start(), calls=%async_computation.4 | async-start | bytes 1179648 | tf_op jit(solution)/shard_map/all_gather | solution.py:114
  6.5 35.2 %collective-permute-start = (bf16[256,1,128]{2,0,1:T(8,128)(2,1)}, bf16[256,1,128]{2,0,1:T(8,128)(2,1)S(1)}, u32[]{:S(2)}, u32[]{:S(2)}) collective-permute-start(bf16[256,1,128]{2,0,1:T(8,128)(2,1)} %param.22), channel_id=1, source_target_pairs={{0,4},{4,8},{8,12},{12,16},{16,20},{20,24},{24,28},{28,0},{1,5},{5... | collective-permute-start | bytes 196616 | tf_op jit(solution)/shard_map/ppermute | solution.py:109
  41.8 33.8 %collective-permute-start.1 = (bf16[256,1,128]{2,0,1:T(8,128)(2,1)S(1)}, bf16[256,1,128]{2,0,1:T(8,128)(2,1)S(1)}, u32[]{:S(2)}, u32[]{:S(2)}) collective-permute-start(bf16[256,1,128]{2,0,1:T(8,128)(2,1)S(1)} %collective-permute-done), channel_id=1, source_target_pairs={{0,4},{4,8},{8,12},{12,16},{16,20},{20,24},{24,28},{28,0},{1,5},{5... | collective-permute-start | bytes 196616 | tf_op jit(solution)/shard_map/ppermute | solution.py:109
  75.5 7.0 %collective-permute-start.2 = (bf16[256,1,128]{2,0,1:T(8,128)(2,1)S(1)}, bf16[256,1,128]{2,0,1:T(8,128)(2,1)S(1)}, u32[]{:S(2)}, u32[]{:S(2)}) collective-permute-start(bf16[256,1,128]{2,0,1:T(8,128)(2,1)S(1)} %collective-permute-done.1), channel_id=1, source_target_pairs={{0,4},{4,8},{8,12},{12,16},{16,20},{20,24},{24,28},{28,0},{1,5},{5... | collective-permute-start | bytes 196616 | tf_op jit(solution)/shard_map/ppermute | solution.py:109
  82.5 7.0 %collective-permute-start.3 = (bf16[256,1,128]{2,0,1:T(8,128)(2,1)S(1)}, bf16[256,1,128]{2,0,1:T(8,128)(2,1)S(1)}, u32[]{:S(2)}, u32[]{:S(2)}) collective-permute-start(bf16[256,1,128]{2,0,1:T(8,128)(2,1)S(1)} %collective-permute-done.2), channel_id=1, source_target_pairs={{0,4},{4,8},{8,12},{12,16},{16,20},{20,24},{24,28},{28,0},{1,5},{5... | collective-permute-start | bytes 196616 | tf_op jit(solution)/shard_map/ppermute | solution.py:109
  89.5 7.1 %collective-permute-start.4 = (bf16[256,1,128]{2,0,1:T(8,128)(2,1)S(1)}, bf16[256,1,128]{2,0,1:T(8,128)(2,1)}, u32[]{:S(2)}, u32[]{:S(2)}) collective-permute-start(bf16[256,1,128]{2,0,1:T(8,128)(2,1)S(1)} %collective-permute-done.3), channel_id=1, source_target_pairs={{0,4},{4,8},{8,12},{12,16},{16,20},{20,24},{24,28},{28,0},{1,5},{5... | collective-permute-start | bytes 196616 | tf_op jit(solution)/shard_map/ppermute | solution.py:109
  96.6 7.3 %collective-permute-start.5 = (bf16[256,1,128]{2,0,1:T(8,128)(2,1)}, bf16[256,1,128]{2,0,1:T(8,128)(2,1)}, u32[]{:S(2)}, u32[]{:S(2)}) collective-permute-start(bf16[256,1,128]{2,0,1:T(8,128)(2,1)} %collective-permute-done.4), channel_id=1, source_target_pairs={{0,4},{4,8},{8,12},{12,16},{16,20},{20,24},{24,28},{28,0},{1,5},{5... | collective-permute-start | bytes 196616 | tf_op jit(solution)/shard_map/ppermute | solution.py:109
  97.9 16.8 %copy-start.11 = (bf16[256,1,128]{2,0,1:T(8,128)(2,1)S(1)}, bf16[256,1,128]{2,0,1:T(8,128)(2,1)}, u32[]{:S(2)}) copy-start(bf16[256,1,128]{2,0,1:T(8,128)(2,1)} %param.21) | copy-start | bytes 196612
  103.8 7.2 %collective-permute-start.6 = (bf16[256,1,128]{2,0,1:T(8,128)(2,1)}, bf16[256,1,128]{2,0,1:T(8,128)(2,1)S(1)}, u32[]{:S(2)}, u32[]{:S(2)}) collective-permute-start(bf16[256,1,128]{2,0,1:T(8,128)(2,1)} %collective-permute-done.5), channel_id=1, source_target_pairs={{0,4},{4,8},{8,12},{12,16},{16,20},{20,24},{24,28},{28,0},{1,5},{5... | collective-permute-start | bytes 196616 | tf_op jit(solution)/shard_map/ppermute | solution.py:109
  116.5 1.9 copy-start.10
  118.5 3.5 %copy-start.2 = (f32[256,2048]{0,1:T(8,128)S(1)}, f32[256,2048]{0,1:T(8,128)}, u32[]{:S(2)}) copy-start(f32[256,2048]{0,1:T(8,128)} %get-tuple-element.62) | copy-start | bytes 6291460
  120.2 1.8 copy-start.1
  125.3 0.7 copy-start.8
  125.9 17.1 %copy-start.5 = (bf16[64,2048]{1,0:T(8,128)(2,1)S(1)}, bf16[64,2048]{1,0:T(8,128)(2,1)}, u32[]{:S(2)}) copy-start(bf16[64,2048]{1,0:T(8,128)(2,1)} %param.20) | copy-start | bytes 786436
  128.1 7.4 %all-to-all-start.1 = ((bf16[4,2,4096]{2,1,0:T(2,128)(2,1)}), bf16[4,2,4096]{2,1,0:T(2,128)(2,1)S(1)}, u32[]{:S(2)}, u32[]{:S(2)}) async-start(bf16[4,2,4096]{2,1,0:T(2,128)(2,1)} %reshape.432), calls=%async_computation.1 | async-start | bytes 131072 | tf_op jit(solution)/shard_map/all_to_all | solution.py:145
  135.5 7.4 %all-to-all-start = ((bf16[4,2,4096]{2,1,0:T(2,128)(2,1)}), bf16[4,2,4096]{2,1,0:T(2,128)(2,1)S(1)}, u32[]{:S(2)}, u32[]{:S(2)}) async-start(bf16[4,2,4096]{2,1,0:T(2,128)(2,1)} %reshape.434), calls=%async_computation | async-start | bytes 131072 | tf_op jit(solution)/shard_map/all_to_all | solution.py:144
  143.1 3.2 copy-start.6
  196.6 53.2 %copy-start.9 = (bf16[1,2048,1024]{2,1,0:T(8,128)(2,1)S(1)}, bf16[1,2048,1024]{2,1,0:T(8,128)(2,1)}, u32[]{:S(2)}) copy-start(bf16[1,2048,1024]{2,1,0:T(8,128)(2,1)} %param.34) | copy-start | bytes 12582916
  248.5 1.3 copy-start.3
  264.0 3.7 %copy-start.7 = (f32[64,4]{0,1:T(4,128)S(1)}, f32[64,4]{0,1:T(4,128)}, u32[]{:S(2)}) copy-start(f32[64,4]{0,1:T(4,128)} %param.33) | copy-start | bytes 3076
  264.0 52.4 %all-to-all-start.3 = ((bf16[32,16,2048]{2,1,0:T(8,128)(2,1)}), bf16[32,16,2048]{2,1,0:T(8,128)(2,1)}, u32[]{:S(2)}, u32[]{:S(2)}) async-start(bf16[32,16,2048]{2,1,0:T(8,128)(2,1)} %bitcast.178), calls=%async_computation.3 | async-start | bytes 4194304 | tf_op jit(solution)/shard_map/all_to_all | solution.py:182
Sparse Core Ops, SparseCore 0:
  9.7 46.0 all-gather.1
